TPU v7x, 32 devices: a whole 2x2x4 slice. The times are simulated.
32 devices in a mesh: sp: 16 (over z, y, x), tp: 2 (over core).
Axes of the slice: x: 2, y: 2, z: 4, core: 2. Of those that a mesh axis runs over, the one named last changes fastest.
Arguments:
- stream: bfloat16 [4096, 2048], P('sp', 'tp'), may hold values from -80 to 80
- norm_gain: float32 [2048], P('tp'), may hold values from 0.1 to 1.9
- cotangent: bfloat16 [4096, 2048], P('sp', 'tp'), may hold values from -6 to 6
- route_weights: float32 [4096, 2], P('sp'), may hold values from 0.1 to 1.5
- routes: int32 [4096, 2], P('sp'), may hold values from 0 to 15, all different within a row; in each aligned block of 256 rows (0 to 255, 256 to 511, ...) at most 64 rows name the same one
- conv_input: bfloat16 [4096, 1024], P('sp', 'tp'), may hold values from -6 to 6
- conv_bgate: bfloat16 [4096, 1024], P('sp', 'tp'), may hold values from -6 to 6
- conv_cgate: bfloat16 [4096, 1024], P('sp', 'tp'), may hold values from -6 to 6
- conv_taps: float32 [3, 1024], P(None, 'tp'), may hold values from -3 to 3
- out_proj: bfloat16 [2048, 1024], P(None, 'tp'), may hold values from -0.1875 to 0.1875
- gate_weight: bfloat16 [16, 2048, 1024], P('sp', None, 'tp'), may hold values from -0.125 to 0.125
- up_weight: bfloat16 [16, 2048, 1024], P('sp', None, 'tp'), may hold values from -0.125 to 0.125
- down_weight: bfloat16 [16, 1024, 2048], P('sp', 'tp'), may hold values from -0.1875 to 0.1875
Outputs:
- stream_grad: bfloat16 [4096, 2048], P('sp', 'tp')
- proj_grad: float32 [2048, 1024], P('sp', 'tp')
- input_grad: bfloat16 [4096, 1024], P('sp', 'tp')
- bgate_grad: bfloat16 [4096, 1024], P('sp', 'tp')
- cgate_grad: bfloat16 [4096, 1024], P('sp', 'tp')
- gate_grad: float32 [16, 2048, 1024], P('sp', None, 'tp')
- up_grad: float32 [16, 2048, 1024], P('sp', None, 'tp')
- down_grad: float32 [16, 1024, 2048], P('sp', 'tp')
Inputs may be any that keep to these rules, and one draw needn't show every extreme that they name: `routes`: the 2 experts of a token differ. Among the tokens of one index of sp, no expert is named more than 64 times, a bound that some block reaches.
All inputs are finite; a program needn't handle non-finite values.
Results may differ from a plain program's by a relative error of at most 0.003.
The roundings to bfloat16 on the way count: a program that leaves them out, or rounds other values in their place, can miss the bound.
Values may be sent and summed in bfloat16 or wider, within the bound.
A program may use at most 128 MiB of HBM per device.

v0:
```python
import jax
import jax.numpy as jnp
from jax import lax
from jax.sharding import PartitionSpec as P

D = 2048


EPSILON = 1e-06


def shifted(value, axis, steps):
    count = lax.axis_size(axis)
    leading, last = (max(0, -steps), min(count, count - steps))
    return lax.ppermute(value, axis, [(source, source + steps) for source in range(leading, last)])


def slot_matrix(routes, experts, capacity):
    assigned = routes.reshape(-1)
    onehot = (assigned[:, None] == jnp.arange(experts, dtype=jnp.int32)[None, :]).astype(jnp.int32)
    earlier = jnp.cumsum(onehot, axis=0) - onehot
    position = jnp.sum(earlier * onehot, axis=1)
    target = assigned * capacity + position
    places = jnp.arange(experts * capacity, dtype=jnp.int32)
    return (places[:, None] == target[None, :]).astype(jnp.bfloat16)


def select_rows(selector, values):
    return jnp.dot(selector, values, preferred_element_type=jnp.float32).astype(jnp.bfloat16)


def contract_rows(left, right):
    return lax.dot_general(
        left, right, (((0,), (0,)), ((), ())), preferred_element_type=jnp.float32
    )


def contract_cols(left, right):
    return lax.dot_general(
        left, right, (((1,), (1,)), ((), ())), preferred_element_type=jnp.float32
    )


def local(
    stream,
    norm_gain,
    cotangent,
    route_weights,
    routes,
    conv_input,
    conv_bgate,
    conv_cgate,
    conv_taps,
    out_proj,
    gate_weight,
    up_weight,
    down_weight,
):
    experts = lax.axis_size("sp")
    tok_count = stream.shape[0]
    top_count = routes.shape[1]
    capacity = 2 * tok_count * top_count // experts
    stream_float = stream.astype(jnp.float32)
    square_sum = lax.psum(jnp.sum(stream_float * stream_float, axis=1), "tp")
    inverse = lax.rsqrt(square_sum / D + EPSILON)[:, None]
    gain_row = norm_gain[None, :]
    normed = (stream_float * inverse * gain_row).astype(jnp.bfloat16)
    cot_float = cotangent.astype(jnp.float32)
    weighted = (route_weights[:, :, None] * cot_float[:, None, :]).astype(jnp.bfloat16)
    weighted = weighted.reshape(tok_count * top_count, -1)
    selector = slot_matrix(routes, experts, capacity)
    token_select = jnp.sum(selector.reshape(experts * capacity, tok_count, top_count), axis=2)
    send_inputs = select_rows(token_select, normed)
    send_grads = select_rows(selector, weighted)
    half_inputs, half_grads = (
        lax.all_to_all(send_inputs, "sp", split_axis=0, concat_axis=0, tiled=True),
        lax.all_to_all(send_grads, "sp", split_axis=0, concat_axis=0, tiled=True),
    )
    recv_inputs, recv_grads = (
        lax.all_gather(half_inputs, "tp", axis=1, tiled=True),
        lax.all_gather(half_grads, "tp", axis=1, tiled=True),
    )
    gate_w = gate_weight[0]
    up_w = up_weight[0]
    down_w = down_weight[0]
    gate_lin = jnp.dot(recv_inputs, gate_w, preferred_element_type=jnp.float32)
    up_lin = jnp.dot(recv_inputs, up_w, preferred_element_type=jnp.float32)
    sigmoid_gate = jax.nn.sigmoid(gate_lin)
    silu_gate = gate_lin * sigmoid_gate
    hidden = (silu_gate * up_lin).astype(jnp.bfloat16)
    down_g = contract_rows(hidden, recv_grads)
    hidden_grad = contract_cols(recv_grads, down_w)
    gate_pre = (
        hidden_grad * up_lin * sigmoid_gate * (1.0 + gate_lin * (1.0 - sigmoid_gate))
    ).astype(jnp.bfloat16)
    up_pre = (hidden_grad * silu_gate).astype(jnp.bfloat16)
    gate_g = contract_rows(recv_inputs, gate_pre)
    up_g = contract_rows(recv_inputs, up_pre)
    partial_value = contract_cols(gate_pre, gate_w) + contract_cols(up_pre, up_w)
    rounded = lax.optimization_barrier(partial_value.astype(jnp.bfloat16))
    summed = lax.psum_scatter(
        rounded.astype(jnp.float32).astype(jnp.bfloat16), "tp", scatter_dimension=1, tiled=True
    )
    returned = lax.all_to_all(summed, "sp", split_axis=0, concat_axis=0, tiled=True)
    normed_grad = contract_rows(token_select, returned)
    cross = lax.psum(jnp.sum(stream_float * gain_row * normed_grad, axis=1), "tp")
    stream_grad = (
        cot_float
        + inverse * gain_row * normed_grad
        - stream_float * inverse * inverse * inverse * cross[:, None] / D
    ).astype(jnp.bfloat16)
    grad_whole = lax.all_gather(stream_grad, "tp", axis=1, tiled=True)
    input_float = conv_input.astype(jnp.float32)
    cgate_float = conv_cgate.astype(jnp.float32)
    bgate_float = conv_bgate.astype(jnp.float32)
    rim_rows = shifted(jnp.stack([conv_input[-2:], conv_cgate[-2:]]), "sp", 1)
    rim_gated = rim_rows[1].astype(jnp.float32) * rim_rows[0].astype(jnp.float32)
    gated = cgate_float * input_float
    extended = jnp.concatenate([rim_gated, gated], axis=0)
    conv_out = (
        conv_taps[0][None, :] * extended[:-2]
        + conv_taps[1][None, :] * extended[1:-1]
        + conv_taps[2][None, :] * extended[2:]
    )
    mixer_out = (bgate_float * conv_out).astype(jnp.bfloat16)
    proj_grad = lax.psum_scatter(
        contract_rows(grad_whole, mixer_out), "sp", scatter_dimension=0, tiled=True
    )
    mixer_grad = jnp.dot(grad_whole, out_proj, preferred_element_type=jnp.float32)
    delta = mixer_grad * bgate_float
    next_rim = shifted(delta[:2], "sp", -1)
    extended_back = jnp.concatenate([delta, next_rim], axis=0)
    gated_grad = (
        conv_taps[2][None, :] * extended_back[:-2]
        + conv_taps[1][None, :] * extended_back[1:-1]
        + conv_taps[0][None, :] * extended_back[2:]
    )
    bgate_grad = (mixer_grad * conv_out).astype(jnp.bfloat16)
    input_grad = (gated_grad * cgate_float).astype(jnp.bfloat16)
    cgate_grad = (gated_grad * input_float).astype(jnp.bfloat16)
    return (
        stream_grad,
        proj_grad,
        input_grad,
        bgate_grad,
        cgate_grad,
        gate_g[None],
        up_g[None],
        down_g[None],
    )


def solution(mesh):
    return jax.shard_map(
        local,
        mesh=mesh,
        in_specs=(
            P("sp", "tp"),
            P("tp"),
            P("sp", "tp"),
            P("sp", None),
            P("sp", None),
            P("sp", "tp"),
            P("sp", "tp"),
            P("sp", "tp"),
            P(None, "tp"),
            P(None, "tp"),
            P("sp", None, "tp"),
            P("sp", None, "tp"),
            P("sp", "tp", None),
        ),
        out_specs=(
            P("sp", "tp"),
            P("sp", "tp"),
            P("sp", "tp"),
            P("sp", "tp"),
            P("sp", "tp"),
            P("sp", None, "tp"),
            P("sp", None, "tp"),
            P("sp", "tp", None),
        ),
        check_vma=False,
    )
```

profile of v0, /device:TPU:0, one launch (start us, length us, event | category | flops | bytes accessed | tf_op | source)
XLA Modules:
  0.0 350.5 jit_solution(6139803511152701945)
XLA Ops:
  7.2 1.0 copy.35
  8.2 0.1 eq.46
  8.3 0.1 eq.50
  8.5 1.2 fusion.21
  9.7 2.6 psum.14
  12.3 1.2 reduce-window.6
  13.5 0.2 slice_reduce_fusion
  13.7 0.1 fusion.48
  13.8 0.1 reduce_sum.43
  14.0 0.1 copy.38
  14.1 0.7 multiply_add_fusion.1
  14.8 0.5 fusion.24
  15.2 2.8 convolution_convert_fusion
  18.1 8.4 %all-to-all-start.1 = ((bf16[16,64,1024]{2,1,0:T(8,128)(2,1)}), bf16[16,64,1024]{2,1,0:T(8,128)(2,1)}, u32[]{:S(2)}, u32[]{:S(2)}) async-start(bf16[16,64,1024]{2,1,0:T(8,128)(2,1)} %bitcast.73), calls=%async_computation.1 | async-start | bytes 4194304 | tf_op jit(solution)/shard_map/all_to_all | solution.py:76
  26.5 0.1 copy.39
  26.7 0.1 mul.202
  26.8 2.9 mul.204
  29.7 3.6 %mul.205 = f32[512,1024]{1,0:T(8,128)} reshape(f32[256,2,1024]{2,1,0:T(2,128)} %mul.204) | data formatting | bytes 4194304 | tf_op jit(solution)/shard_map/mul | solution.py:69
  33.4 36.4 %all-to-all-done.1 = bf16[16,64,1024]{2,1,0:T(8,128)(2,1)} async-done(((bf16[16,64,1024]{2,1,0:T(8,128)(2,1)}), bf16[16,64,1024]{2,1,0:T(8,128)(2,1)}, u32[]{:S(2)}, u32[]{:S(2)}) %all-to-all-start.1) | async-done | bytes 2097184 | tf_op jit(solution)/shard_map/all_to_all | solution.py:76
  69.8 0.0 all-gather.4.cloned.1.call-start
  69.8 2.9 fusion.12
  72.7 58.3 %all_to_all.36 = bf16[16,64,1024]{2,1,0:T(8,128)(2,1)} all-to-all(bf16[16,64,1024]{2,1,0:T(8,128)(2,1)S(1)} %bitcast.75), channel_id=1, replica_groups=mesh['sp'=16,'tp'=2] {'sp'}, dimensions={0} | all-to-all | bytes 4194304 | tf_op jit(solution)/shard_map/all_to_all | solution.py:77
  131.1 0.2 reduce-scatter.3.cloned.1.call-start
  131.4 6.0 %fusion.2 = f32[1024,512]{1,0:T(8,128)} fusion(bf16[1024,2048]{1,0:T(8,128)(2,1)} %all-gather.6.cloned.1.call-done, bf16[1,2048,512]{2,1,0:T(8,128)(2,1)S(1)} %copy-done), kind=kOutput, calls=%fused_computation.6 | convolution fusion | flops 2147483648 | bytes 8388608 | tf_op jit(solution)/shard_map/dot_general | solution.py:86
  137.4 3.7 %fusion.5 = f32[1024,512]{1,0:T(8,128)} fusion(bf16[1024,2048]{1,0:T(8,128)(2,1)S(1)} %copy-done.12, bf16[1,2048,512]{2,1,0:T(8,128)(2,1)S(1)} %copy-done.15), kind=kOutput, calls=%fused_computation.9 | convolution fusion | flops 2147483648 | bytes 8388608 | tf_op jit(solution)/shard_map/dot_general | solution.py:87
  141.0 2.3 all-gather.4.cloned.1.call-done
  143.3 7.0 %multiply_convert_fusion.1 = (bf16[1024,512]{1,0:T(8,128)(2,1)S(1)}, bf16[1024,512]{1,0:T(8,128)(2,1)S(1)}) fusion(f32[1024,512]{1,0:T(8,128)} %fusion.2, f32[1024,512]{1,0:T(8,128)} %fusion.5, bf16[1024,2048]{1,0:T(8,128)(2,1)} %all-gather.4.cloned.1.call-done, bf16[1,512,2048]{2,1,0:T(8,128)(2,1)} %param.25), kind=kOutput, calls=%fused_computation.14 | convolution fusion | flops 2154299392 | bytes 12582912 | tf_op jit(solution)/shard_map/dot_general | solution.py:39
  150.4 2.4 fusion
  152.8 4.4 %add_convert_fusion = bf16[1024,2048]{1,0:T(8,128)(2,1)} fusion(f32[1024,2048]{1,0:T(8,128)S(1)} %fusion, bf16[1024,512]{1,0:T(8,128)(2,1)S(1)} %get-tuple-element.12, bf16[1,2048,512]{2,1,0:T(8,128)(2,1)S(1)} %copy-done.16), kind=kOutput, calls=%fused_computation | convolution fusion | flops 2151677952 | bytes 15728640 | tf_op jit(solution)/shard_map/dot_general | solution.py:39
  157.3 13.2 %reduce-scatter.3.cloned.1.call-done = bf16[1024,1024]{1,0:T(8,128)(2,1)} async-done(((bf16[1024,2048]{1,0:T(8,128)(2,1)}), bf16[1024,1024]{1,0:T(8,128)(2,1)}) %reduce-scatter.3.cloned.1.call-update) | async-done | bytes 2097168 | tf_op jit(solution)/shard_map/reduce_scatter | solution.py:101
  170.4 56.1 %all_to_all.37 = bf16[16,64,1024]{2,1,0:T(8,128)(2,1)S(1)} all-to-all(bf16[16,64,1024]{2,1,0:T(8,128)(2,1)} %bitcast.74), channel_id=1, replica_groups=mesh['sp'=16,'tp'=2] {'sp'}, dimensions={0} | all-to-all | bytes 4194304 | tf_op jit(solution)/shard_map/all_to_all | solution.py:104
  226.6 1.7 fusion.23
  228.3 2.6 psum.15
  230.9 2.6 fusion.20
  233.6 2.7 collective-permute-start
  236.3 0.1 convert_multiply_fusion.4
  236.4 1.0 collective-permute-done
  237.4 3.6 %all-gather.8.cloned.1.call-done = bf16[256,2048]{1,0:T(8,128)(2,1)} async-done(((bf16[256,1024]{1,0:T(8,128)(2,1)}), bf16[256,2048]{1,0:T(8,128)(2,1)}) %all-gather.8.cloned.1.call-update) | async-done | bytes 1048592 | tf_op jit(solution)/shard_map/all_gather | solution.py:112
  241.1 3.5 multiply_convert_fusion.6
  244.6 2.7 fusion.44
  247.3 1.2 copy-done.18
  248.5 6.7 %convolution_bitcast_fusion.1 = f32[1,2048,512]{2,1,0:T(8,128)} fusion(bf16[1024,2048]{1,0:T(8,128)(2,1)} %all-gather.6.cloned.1.call-done, bf16[1024,512]{1,0:T(8,128)(2,1)S(1)} %copy-done.18), kind=kOutput, calls=%fused_computation.2 | convolution fusion | flops 2147483648 | bytes 9437184 | tf_op jit(solution)/shard_map/dot_general | solution.py:33
  255.3 4.6 %convolution_bitcast_fusion = f32[1,512,2048]{2,1,0:T(8,128)} fusion(bf16[1024,2048]{1,0:T(8,128)(2,1)S(1)} %copy-done.14, f32[1024,512]{1,0:T(8,128)S(1)} %copy-done.22, f32[1024,512]{1,0:T(8,128)S(1)} %copy-done.21), kind=kOutput, calls=%fused_computation.1 | convolution fusion | flops 2150629376 | bytes 12582912 | tf_op jit(solution)/shard_map/dot_general | solution.py:33
  259.9 1.4 collective-permute-start.1
  261.3 4.5 %convolution_bitcast_fusion.2 = f32[1,2048,512]{2,1,0:T(8,128)} fusion(bf16[1024,2048]{1,0:T(8,128)(2,1)S(1)} %copy-done.13, bf16[1024,512]{1,0:T(8,128)(2,1)S(1)} %copy-done.20), kind=kOutput, calls=%fused_computation.3 | convolution fusion | flops 2147483648 | bytes 9437184 | tf_op jit(solution)/shard_map/dot_general | solution.py:33
  265.8 0.9 fusion.37
  266.7 0.8 fusion.36
  267.5 76.5 %reduce-scatter.5.cloned.1.call-done = f32[128,512]{1,0:T(8,128)} async-done(((f32[2048,512]{1,0:T(8,128)}), f32[128,512]{1,0:T(8,128)}) %reduce-scatter.5.cloned.1.call-update) | async-done | bytes 262160 | tf_op jit(solution)/shard_map/reduce_scatter | solution.py:126
  (65 shorter events, 0.4 us)
Async XLA Ops:
  7.2 124.2 %copy-start = (bf16[1,2048,512]{2,1,0:T(8,128)(2,1)S(1)}, bf16[1,2048,512]{2,1,0:T(8,128)(2,1)}, u32[]{:S(2)}) copy-start(bf16[1,2048,512]{2,1,0:T(8,128)(2,1)} %param.23) | copy-start | bytes 6291460
  7.2 8.1 %copy-start.2 = (bf16[256,1024]{1,0:T(8,128)(2,1)S(1)}, bf16[256,1024]{1,0:T(8,128)(2,1)}, u32[]{:S(2)}) copy-start(bf16[256,1024]{1,0:T(8,128)(2,1)} %param.13) | copy-start | bytes 1572868
  18.1 8.4 %copy-start.11 = (f32[256,2]{0,1:T(2,128)S(1)}, f32[256,2]{0,1:T(2,128)}, u32[]{:S(2)}) copy-start(f32[256,2]{0,1:T(2,128)} %param.16) | copy-start | bytes 6148
  18.1 51.7 %all-to-all-start.1 = ((bf16[16,64,1024]{2,1,0:T(8,128)(2,1)}), bf16[16,64,1024]{2,1,0:T(8,128)(2,1)}, u32[]{:S(2)}, u32[]{:S(2)}) async-start(bf16[16,64,1024]{2,1,0:T(8,128)(2,1)} %bitcast.73), calls=%async_computation.1 | async-start | bytes 4194304 | tf_op jit(solution)/shard_map/all_to_all | solution.py:76
  26.5 104.9 %all-gather.6.cloned.1.call-start = ((), (), s32[]{:S(2)}) async-start(), calls=%async_computation.6 | async-start | bytes 6291456 | tf_op jit(solution)/shard_map/all_gather | solution.py:80
  69.8 73.5 %all-gather.4.cloned.1.call-start = ((), (), s32[]{:S(2)}) async-start(), calls=%async_computation.5 | async-start | bytes 6291456 | tf_op jit(solution)/shard_map/all_gather | solution.py:81
  131.1 39.3 %reduce-scatter.3.cloned.1.call-start = ((), (), s32[]{:S(2)}) async-start(), calls=%async_computation.7 | async-start | bytes 6291456 | tf_op jit(solution)/shard_map/reduce_scatter | solution.py:101
  131.3 6.0 %copy-start.12 = (bf16[1024,2048]{1,0:T(8,128)(2,1)S(1)}, bf16[1024,2048]{1,0:T(8,128)(2,1)}, u32[]{:S(2)}) copy-start(bf16[1024,2048]{1,0:T(8,128)(2,1)} %all-gather.6.cloned.1.call-done) | copy-start | bytes 12582916
  131.3 6.0 %copy-start.15 = (bf16[1,2048,512]{2,1,0:T(8,128)(2,1)S(1)}, bf16[1,2048,512]{2,1,0:T(8,128)(2,1)}, u32[]{:S(2)}) copy-start(bf16[1,2048,512]{2,1,0:T(8,128)(2,1)} %param.24) | copy-start | bytes 6291460
  150.4 2.4 copy-start.19
  150.4 2.4 copy-start.17
  150.4 2.4 copy-start.16
  157.2 83.8 %all-gather.8.cloned.1.call-start = ((), (), s32[]{:S(2)}) async-start(), calls=%async_computation.8 | async-start | bytes 1572864 | tf_op jit(solution)/shard_map/all_gather | solution.py:112
  170.4 56.1 %copy-start.9 = (f32[1024]{0:T(1024)S(1)}, f32[1024]{0:T(1024)}, u32[]{:S(2)}) copy-start(f32[1024]{0:T(1024)} %param.14) | copy-start | bytes 12292
  228.3 5.3 %copy-start.4 = (bf16[256,512]{1,0:T(8,128)(2,1)S(1)}, bf16[256,512]{1,0:T(8,128)(2,1)}, u32[]{:S(2)}) copy-start(bf16[256,512]{1,0:T(8,128)(2,1)} %param.18) | copy-start | bytes 786436
  228.3 5.3 %copy-start.5 = (bf16[256,512]{1,0:T(8,128)(2,1)S(1)}, bf16[256,512]{1,0:T(8,128)(2,1)}, u32[]{:S(2)}) copy-start(bf16[256,512]{1,0:T(8,128)(2,1)} %param.20) | copy-start | bytes 786436
  230.9 5.6 %copy-start.10 = (f32[3,512]{1,0:T(4,128)S(1)}, f32[3,512]{1,0:T(4,128)}, u32[]{:S(2)}) copy-start(f32[3,512]{1,0:T(4,128)} %param.21) | copy-start | bytes 18436
  230.9 10.2 %copy-start.8 = (bf16[256,512]{1,0:T(8,128)(2,1)S(1)}, bf16[256,512]{1,0:T(8,128)(2,1)}, u32[]{:S(2)}) copy-start(bf16[256,512]{1,0:T(8,128)(2,1)} %param.19) | copy-start | bytes 786436
  233.5 110.5 %reduce-scatter.5.cloned.1.call-start = ((), (), s32[]{:S(2)}) async-start(), calls=%async_computation.9 | async-start | bytes 4456448 | tf_op jit(solution)/shard_map/reduce_scatter | solution.py:126
  233.6 3.8 %collective-permute-start = (bf16[2,2,512]{2,1,0:T(2,128)(2,1)S(1)}, bf16[2,2,512]{2,1,0:T(2,128)(2,1)S(1)}, u32[]{:S(2)}, u32[]{:S(2)}) collective-permute-start(bf16[2,2,512]{2,1,0:T(2,128)(2,1)S(1)} %pad_maximum_fusion.2), channel_id=1, source_target_pairs={{0,2},{2,4},{4,6},{6,8},{8,10},{10,12},{12,14},{14,16},{16,18},{18... | collective-permute-start | bytes 12296 | tf_op jit(solution)/shard_map/ppermute | solution.py:15
  241.1 3.5 copy-start.3
  244.6 15.3 %copy-start.6 = (f32[256,512]{1,0:T(8,128)}, f32[256,512]{1,0:T(8,128)S(1)}, u32[]{:S(2)}) copy-start(f32[256,512]{1,0:T(8,128)S(1)} %get-tuple-element.14) | copy-start | bytes 1572868
  247.3 1.2 copy-start.18
  248.5 6.7 %copy-start.14 = (bf16[1024,2048]{1,0:T(8,128)(2,1)S(1)}, bf16[1024,2048]{1,0:T(8,128)(2,1)}, u32[]{:S(2)}) copy-start(bf16[1024,2048]{1,0:T(8,128)(2,1)} %all-gather.4.cloned.1.call-done) | copy-start | bytes 12582916
  248.5 6.7 %copy-start.21 = (f32[1024,512]{1,0:T(8,128)S(1)}, f32[1024,512]{1,0:T(8,128)}, u32[]{:S(2)}) copy-start(f32[1024,512]{1,0:T(8,128)} %fusion.2) | copy-start | bytes 6291460
  248.5 6.7 %copy-start.22 = (f32[1024,512]{1,0:T(8,128)S(1)}, f32[1024,512]{1,0:T(8,128)}, u32[]{:S(2)}) copy-start(f32[1024,512]{1,0:T(8,128)} %fusion.5) | copy-start | bytes 6291460
  255.2 6.0 %copy-start.13 = (bf16[1024,2048]{1,0:T(8,128)(2,1)S(1)}, bf16[1024,2048]{1,0:T(8,128)(2,1)}, u32[]{:S(2)}) copy-start(bf16[1024,2048]{1,0:T(8,128)(2,1)} %all-gather.6.cloned.1.call-done) | copy-start | bytes 12582916
  255.2 6.0 %copy-start.20 = (bf16[1024,512]{1,0:T(8,128)(2,1)S(1)}, bf16[1024,512]{1,0:T(8,128)(2,1)}, u32[]{:S(2)}) copy-start(bf16[1024,512]{1,0:T(8,128)(2,1)} %copy-done.19) | copy-start | bytes 3145732
  259.9 5.9 %copy-start.7 = (f32[256,512]{1,0:T(8,128)S(1)}, f32[256,512]{1,0:T(8,128)}, u32[]{:S(2)}) copy-start(f32[256,512]{1,0:T(8,128)} %copy-done.6) | copy-start | bytes 1572868
  259.9 5.9 %collective-permute-start.1 = (f32[2,512]{1,0:T(2,128)S(1)}, f32[2,512]{1,0:T(2,128)S(1)}, u32[]{:S(2)}, u32[]{:S(2)}) collective-permute-start(f32[2,512]{1,0:T(2,128)S(1)} %slice.64), channel_id=1, source_target_pairs={{2,0},{4,2},{6,4},{8,6},{10,8},{12,10},{14,12},{16,14},{18,16},{20... | collective-permute-start | bytes 12296 | tf_op jit(solution)/shard_map/ppermute | solution.py:15
  261.3 82.7 %copy-start.1 = (bf16[1,2048,512]{2,1,0:T(8,128)(2,1)S(1)}, bf16[1,2048,512]{2,1,0:T(8,128)(2,1)}, u32[]{:S(2)}) copy-start(bf16[1,2048,512]{2,1,0:T(8,128)(2,1)} %param.23) | copy-start | bytes 6291460
Sparse Core Ops, SparseCore 0:
  69.9 18.2 all-gather.5
  131.2 12.0 all-gather.3
  157.3 13.0 reduce-scatter.2
  233.7 7.3 all-gather.7
  247.4 96.5 reduce-scatter.4
where the time goes:
time: 351 us
  waiting for transfers between devices  133 us (38%)
  blocking collectives  120 us (34%)
  matrix products  52.9 us (15%)
  between operations  14.1 us (4%)
  starting transfers between devices  12.9 us (4%)
  local copies, waits for them, and re-layouts  9.85 us (3%)
  other arithmetic  8.12 us (2%)
    reduce_scatter x1, waiting for transfers between devices, local(): lax.psum_scatter(contract_rows(grad_whole, mixer_out), 'sp', scatter_dime...  76.5 us
    all_to_all x1, blocking collectives, local(): lax.all_to_all(send_grads, 'sp', split_axis=0, concat_axis=0, tiled=True)  58.3 us
    all_to_all x1, blocking collectives, local(): lax.all_to_all(summed, 'sp', split_axis=0, concat_axis=0, tiled=True)  56.1 us
    all_to_all x1, waiting for transfers between devices, local(): lax.all_to_all(send_inputs, 'sp', split_axis=0, concat_axis=0, tiled=True)  36.4 us
    dot_general x5, matrix products, contract_rows(): lax.dot_general(left, right, (((0,), (0,)), ((), ())), preferred_element_...  20.2 us
    dot_general x3, matrix products, contract_cols(): lax.dot_general(left, right, (((1,), (1,)), ((), ())), preferred_element_...  13.8 us
    reduce_scatter x1, waiting for transfers between devices, local(): lax.psum_scatter(rounded.astype(jnp.float32).astype(jnp.bfloat16), 'tp',...  13.2 us
    all_to_all x1, starting transfers between devices, local(): lax.all_to_all(send_inputs, 'sp', split_axis=0, concat_axis=0, tiled=True)  8.36 us
  transfers between devices with their start and end apart: 8, of which 6 were waited for; matrix products, arithmetic and copies ran while one was open for 11% of the time, Pallas kernels for 0%

commit v1 on v0

--- a/solution.py
+++ b/solution.py
@@ -1,6 +1,8 @@
 import jax
 import jax.numpy as jnp
 from jax import lax
+from jax.experimental import pallas as pl
+from jax.experimental.pallas import tpu as pltpu
 from jax.sharding import PartitionSpec as P
 
 D = 2048
@@ -39,6 +41,208 @@
     return lax.dot_general(
         left, right, (((1,), (1,)), ((), ())), preferred_element_type=jnp.float32
     )
+
+
+MESH = pl.DeviceIdType.MESH
+
+
+def greet(count, peer_of, other=None):
+    barrier = pltpu.get_barrier_semaphore()
+
+    @pl.loop(1, count)
+    def _(i):
+        pl.semaphore_signal(barrier, inc=1, device_id={"sp": peer_of(i)}, device_id_type=MESH)
+
+    if other is not None:
+        pl.semaphore_signal(barrier, inc=1, device_id={"tp": other}, device_id_type=MESH)
+    pl.semaphore_wait(barrier, count - 1 if other is None else count)
+
+
+def dispatch_kernel(
+    count,
+    group,
+    x_ref,
+    y_ref,
+    m_ref,
+    ox_ref,
+    oy_ref,
+    om_ref,
+    send,
+    recv,
+    fsend,
+    frecv,
+    msend,
+    mrecv,
+    own,
+):
+    me = lax.axis_index("sp")
+    side = lax.axis_index("tp")
+    other = 1 - side
+    block = x_ref.shape[0] // count
+    width = x_ref.shape[1]
+    mine = pl.ds(pl.multiple_of(side * width, width), width)
+    pairs = ((x_ref, ox_ref), (y_ref, oy_ref))
+
+    def rows(index):
+        return pl.ds(pl.multiple_of(index * block, block), block)
+
+    def ahead(i):
+        return i + side * (count - 2 * i)
+
+    def remote(a, i):
+        src, dst = pairs[a]
+        peer = lax.rem(me + ahead(i), count)
+        return pltpu.make_async_remote_copy(
+            src_ref=src.at[rows(peer)],
+            dst_ref=dst.at[rows(me), mine],
+            send_sem=send.at[a, i],
+            recv_sem=recv.at[a, i],
+            device_id={"sp": peer},
+            device_id_type=MESH,
+        )
+
+    def forward(a, i):
+        dst = pairs[a][1]
+        spot = dst.at[rows(lax.rem(me + count - ahead(i), count)), mine]
+        return pltpu.make_async_remote_copy(
+            src_ref=spot,
+            dst_ref=spot,
+            send_sem=fsend.at[a, i],
+            recv_sem=frecv.at[a, i],
+            device_id={"tp": other},
+            device_id_type=MESH,
+        )
+
+    def home(a):
+        src, dst = pairs[a]
+        return pltpu.make_async_copy(src.at[rows(me)], dst.at[rows(me), mine], own.at[a])
+
+    place = lax.rem(me, group)
+    tokens = m_ref.shape[0]
+    spot_m = om_ref.at[pl.ds(pl.multiple_of(place * tokens, tokens), tokens)]
+
+    def mixer(i):
+        return pltpu.make_async_remote_copy(
+            src_ref=m_ref,
+            dst_ref=spot_m,
+            send_sem=msend.at[i],
+            recv_sem=mrecv.at[i],
+            device_id={"sp": me - place + lax.rem(place + i, group)},
+            device_id_type=MESH,
+        )
+
+    home_m = pltpu.make_async_copy(m_ref, spot_m, own.at[2])
+    greet(count, lambda i: lax.rem(me + i, count), other)
+    for a in range(2):
+
+        @pl.loop(1, count)
+        def _(i):
+            remote(a, i).start()
+
+        home(a).start()
+
+    @pl.loop(1, group)
+    def _(i):
+        mixer(i).start()
+
+    home_m.start()
+    for a in range(2):
+        home(a).wait()
+        forward(a, 0).start()
+
+        @pl.loop(1, count)
+        def _(i):
+            remote(a, i).wait_recv()
+            forward(a, i).start()
+
+    for a in range(2):
+
+        @pl.loop(1, count)
+        def _(i):
+            remote(a, i).wait_send()
+
+        @pl.loop(0, count)
+        def _(i):
+            forward(a, i).wait()
+
+    @pl.loop(1, group)
+    def _(i):
+        mixer(i).wait()
+
+    home_m.wait()
+
+
+def dispatch(x, y, mixed, group):
+    count = lax.axis_size("sp")
+    gathered = jax.ShapeDtypeStruct((group * mixed.shape[0], mixed.shape[1]), mixed.dtype)
+    whole = jax.ShapeDtypeStruct((x.shape[0], 2 * x.shape[1]), x.dtype)
+    return pl.pallas_call(
+        lambda *refs: dispatch_kernel(count, group, *refs),
+        out_shape=(whole, whole, gathered),
+        in_specs=[pl.BlockSpec(memory_space=pltpu.VMEM)] * 3,
+        out_specs=[pl.BlockSpec(memory_space=pltpu.VMEM)] * 3,
+        scratch_shapes=[pltpu.SemaphoreType.DMA((2, count))] * 4
+        + [pltpu.SemaphoreType.DMA((group,))] * 2
+        + [pltpu.SemaphoreType.DMA((3,))],
+        compiler_params=pltpu.CompilerParams(
+            collective_id=0, has_side_effects=True, vmem_limit_bytes=40 * 2**20
+        ),
+        name="dispatch",
+    )(x, y, mixed)
+
+
+def spread_kernel(count, step, x_ref, o_ref, send, recv, own):
+    me = lax.axis_index("sp")
+    side = lax.axis_index("tp")
+    here = lax.rem(lax.div(me, step), count)
+    block = x_ref.shape[0] // count
+
+    def rows(index):
+        return pl.ds(pl.multiple_of(index * block, block), block)
+
+    def slot(i):
+        return lax.rem(here + i + side * (count - 2 * i), count)
+
+    def peer_of(i):
+        return me + (slot(i) - here) * step
+
+    def remote(i):
+        return pltpu.make_async_remote_copy(
+            src_ref=x_ref.at[rows(slot(i))],
+            dst_ref=o_ref.at[rows(here)],
+            send_sem=send.at[i],
+            recv_sem=recv.at[i],
+            device_id={"sp": peer_of(i)},
+            device_id_type=MESH,
+        )
+
+    greet(count, peer_of)
+
+    @pl.loop(1, count)
+    def _(i):
+        remote(i).start()
+
+    home = pltpu.make_async_copy(x_ref.at[rows(here)], o_ref.at[rows(here)], own)
+    home.start()
+    home.wait()
+
+    @pl.loop(1, count)
+    def _(i):
+        remote(i).wait()
+
+
+def spread(x, number, count, step):
+    return pl.pallas_call(
+        lambda *refs: spread_kernel(count, step, *refs),
+        out_shape=jax.ShapeDtypeStruct(x.shape, x.dtype),
+        in_specs=[pl.BlockSpec(memory_space=pltpu.VMEM)],
+        out_specs=pl.BlockSpec(memory_space=pltpu.VMEM),
+        scratch_shapes=[pltpu.SemaphoreType.DMA((count,))] * 2 + [pltpu.SemaphoreType.DMA],
+        compiler_params=pltpu.CompilerParams(
+            collective_id=number, has_side_effects=True, vmem_limit_bytes=24 * 2**20
+        ),
+        name="spread%d" % number,
+    )(x)
 
 
 def local(
@@ -72,14 +276,22 @@
     token_select = jnp.sum(selector.reshape(experts * capacity, tok_count, top_count), axis=2)
     send_inputs = select_rows(token_select, normed)
     send_grads = select_rows(selector, weighted)
-    half_inputs, half_grads = (
-        lax.all_to_all(send_inputs, "sp", split_axis=0, concat_axis=0, tiled=True),
-        lax.all_to_all(send_grads, "sp", split_axis=0, concat_axis=0, tiled=True),
-    )
-    recv_inputs, recv_grads = (
-        lax.all_gather(half_inputs, "tp", axis=1, tiled=True),
-        lax.all_gather(half_grads, "tp", axis=1, tiled=True),
-    )
+    input_float = conv_input.astype(jnp.float32)
+    cgate_float = conv_cgate.astype(jnp.float32)
+    bgate_float = conv_bgate.astype(jnp.float32)
+    rim_rows = shifted(jnp.stack([conv_input[-2:], conv_cgate[-2:]]), "sp", 1)
+    rim_gated = rim_rows[1].astype(jnp.float32) * rim_rows[0].astype(jnp.float32)
+    gated = cgate_float * input_float
+    extended = jnp.concatenate([rim_gated, gated], axis=0)
+    conv_out = (
+        conv_taps[0][None, :] * extended[:-2]
+        + conv_taps[1][None, :] * extended[1:-1]
+        + conv_taps[2][None, :] * extended[2:]
+    )
+    mixer_out = (bgate_float * conv_out).astype(jnp.bfloat16)
+    group = 2 ** ((experts.bit_length() - 1) // 2)
+    stages = experts // group
+    recv_inputs, recv_grads, mixer_near = dispatch(send_inputs, send_grads, mixer_out, group)
     gate_w = gate_weight[0]
     up_w = up_weight[0]
     down_w = down_weight[0]
@@ -96,12 +308,20 @@
     up_pre = (hidden_grad * silu_gate).astype(jnp.bfloat16)
     gate_g = contract_rows(recv_inputs, gate_pre)
     up_g = contract_rows(recv_inputs, up_pre)
-    partial_value = contract_cols(gate_pre, gate_w) + contract_cols(up_pre, up_w)
-    rounded = lax.optimization_barrier(partial_value.astype(jnp.bfloat16))
-    summed = lax.psum_scatter(
-        rounded.astype(jnp.float32).astype(jnp.bfloat16), "tp", scatter_dimension=1, tiled=True
-    )
-    returned = lax.all_to_all(summed, "sp", split_axis=0, concat_axis=0, tiled=True)
+    side = lax.axis_index("tp")
+    half = gate_w.shape[0] // 2
+
+    def partial_of(part):
+        gate_half = lax.dynamic_slice_in_dim(gate_w, part * half, half, axis=0)
+        up_half = lax.dynamic_slice_in_dim(up_w, part * half, half, axis=0)
+        value = contract_cols(gate_pre, gate_half) + contract_cols(up_pre, up_half)
+        return lax.optimization_barrier(value.astype(jnp.bfloat16))
+
+    theirs = lax.ppermute(partial_of(1 - side), "tp", [(0, 1), (1, 0)])
+    summed = (partial_of(side).astype(jnp.float32) + theirs.astype(jnp.float32)).astype(
+        jnp.bfloat16
+    )
+    returned = spread(summed, 1, experts, 1)
     normed_grad = contract_rows(token_select, returned)
     cross = lax.psum(jnp.sum(stream_float * gain_row * normed_grad, axis=1), "tp")
     stream_grad = (
@@ -109,23 +329,20 @@
         + inverse * gain_row * normed_grad
         - stream_float * inverse * inverse * inverse * cross[:, None] / D
     ).astype(jnp.bfloat16)
-    grad_whole = lax.all_gather(stream_grad, "tp", axis=1, tiled=True)
-    input_float = conv_input.astype(jnp.float32)
-    cgate_float = conv_cgate.astype(jnp.float32)
-    bgate_float = conv_bgate.astype(jnp.float32)
-    rim_rows = shifted(jnp.stack([conv_input[-2:], conv_cgate[-2:]]), "sp", 1)
-    rim_gated = rim_rows[1].astype(jnp.float32) * rim_rows[0].astype(jnp.float32)
-    gated = cgate_float * input_float
-    extended = jnp.concatenate([rim_gated, gated], axis=0)
-    conv_out = (
-        conv_taps[0][None, :] * extended[:-2]
-        + conv_taps[1][None, :] * extended[1:-1]
-        + conv_taps[2][None, :] * extended[2:]
-    )
-    mixer_out = (bgate_float * conv_out).astype(jnp.bfloat16)
-    proj_grad = lax.psum_scatter(
-        contract_rows(grad_whole, mixer_out), "sp", scatter_dimension=0, tiled=True
-    )
+    grad_other = lax.ppermute(stream_grad, "tp", [(0, 1), (1, 0)])
+    grad_whole = jnp.concatenate(
+        [
+            jnp.where(side == 0, stream_grad, grad_other),
+            jnp.where(side == 0, grad_other, stream_grad),
+        ],
+        axis=1,
+    )
+    columns = grad_whole.reshape(tok_count, stages, group, -1).transpose(2, 0, 1, 3)
+    grad_near = spread(columns.reshape(group * tok_count, -1), 2, group, 1)
+    shares = contract_rows(grad_near, mixer_near).astype(jnp.bfloat16)
+    shares = spread(shares, 3, stages, group)
+    shares = shares.reshape(stages, shares.shape[0] // stages, -1)
+    proj_grad = jnp.sum(shares.astype(jnp.float32), axis=0)
     mixer_grad = jnp.dot(grad_whole, out_proj, preferred_element_type=jnp.float32)
     delta = mixer_grad * bgate_float
     next_rim = shifted(delta[:2], "sp", -1)

time: 351 us -> 265 us (0.75)
  Pallas kernels: 0 us -> 173 us
  waiting for transfers between devices: 133 us -> 3.44 us
  blocking collectives: 120 us -> 16.6 us
  matrix products: 52.9 us -> 37.2 us
  between operations: 14.1 us -> 1.15 us
  local copies, waits for them, and re-layouts: 9.85 us -> 15.9 us
  starting transfers between devices: 12.9 us -> 6.9 us
    pallas_call x0 -> x4, Pallas kernels: none -> 173 us  [the longest x1 99.7 us: dispatch(): pl.pallas_call(lambda *refs: dispatch_kernel(count, group, *refs), out_sh...]
    all_to_all x2 -> x0, blocking collectives: 114 us -> none  [the longest x1 58.3 us: local(): lax.all_to_all(send_grads, 'sp', split_axis=0, concat_axis=0, tiled=True)]
    reduce_scatter x2 -> x0, waiting for transfers between devices: 89.7 us -> none  [the longest x1 76.5 us: local(): lax.psum_scatter(contract_rows(grad_whole, mixer_out), 'sp', scatter_dime...]
    all_to_all x1 -> x0, waiting for transfers between devices: 36.4 us -> none  [local(): lax.all_to_all(send_inputs, 'sp', split_axis=0, concat_axis=0, tiled=True)]
    psum x1, blocking collectives: 2.58 us -> 14.2 us  [local(): lax.psum(jnp.sum(stream_float * gain_row * normed_grad, axis=1), 'tp')]
    all_to_all x1 -> x0, starting transfers between devices: 8.36 us -> none  [local(): lax.all_to_all(send_inputs, 'sp', split_axis=0, concat_axis=0, tiled=True)]
    all_gather x3 -> x0, waiting for transfers between devices: 5.94 us -> none  [the longest x1 3.62 us: local(): grad_whole = lax.all_gather(stream_grad, 'tp', axis=1, tiled=True)]
    dot_general x3 -> x5, matrix products: 13.8 us -> 8.2 us  [contract_cols(): lax.dot_general(left, right, (((1,), (1,)), ((), ())), preferred_element_...]
  transfers between devices with their start and end apart: 8 -> 4, of which waited for: 6 -> 1; matrix products, arithmetic and copies ran while one was open for 11% -> 14% of each run, Pallas kernels for 0% -> 0%
where the time goes in v1:
time: 265 us
  Pallas kernels  173 us (65%)
  matrix products  37.2 us (14%)
  blocking collectives  16.6 us (6%)
  local copies, waits for them, and re-layouts  15.9 us (6%)
  other arithmetic  10.3 us (4%)
  starting transfers between devices  6.9 us (3%)
  waiting for transfers between devices  3.44 us (1%)
    pallas_call x1, Pallas kernels, dispatch(): pl.pallas_call(lambda *refs: dispatch_kernel(count, group, *refs), out_sh...  99.7 us
    pallas_call x3, Pallas kernels, spread(): pl.pallas_call(lambda *refs: spread_kernel(count, step, *refs), out_shape...  73.3 us
    dot_general x5, matrix products, contract_rows(): lax.dot_general(left, right, (((0,), (0,)), ((), ())), preferred_element_...  18.1 us
    psum x1, blocking collectives, local(): lax.psum(jnp.sum(stream_float * gain_row * normed_grad, axis=1), 'tp')  14.2 us
    dot_general x5, matrix products, contract_cols(): lax.dot_general(left, right, (((1,), (1,)), ((), ())), preferred_element_...  8.2 us
    mul x3, local copies, waits for them, and re-layouts, local(): route_weights[:, :, None] * cot_float[:, None, :]  6.91 us
    ppermute x2, starting transfers between devices, shifted(): lax.ppermute(value, axis, [(source, source + steps) for source in range(l...  6.28 us
    unnamed x63, local copies, waits for them, and re-layouts  6.17 us
  transfers between devices with their start and end apart: 4, of which 1 were waited for; matrix products, arithmetic and copies ran while one was open for 14% of the time, Pallas kernels for 0%

profile of v1, /device:TPU:0, one launch (start us, length us, event | category | flops | bytes accessed | tf_op | source)
XLA Modules:
  0.0 264.5 jit_solution(1862406260526905080)
XLA Ops:
  0.7 0.9 slice_bitcast_fusion
  1.6 4.9 %collective-permute-start = (bf16[2,2,512]{2,1,0:T(2,128)(2,1)S(1)}, bf16[2,2,512]{2,1,0:T(2,128)(2,1)S(1)}, u32[]{:S(2)}, u32[]{:S(2)}) collective-permute-start(bf16[2,2,512]{2,1,0:T(2,128)(2,1)S(1)} %pad_maximum_fusion.3), channel_id=1, source_target_pairs={{0,2},{2,4},{4,6},{6,8},{8,10},{10,12},{12,14},{14,16},{16,18},{18... | collective-permute-start | bytes 12296 | tf_op jit(solution)/shard_map/ppermute | solution.py:17
  6.5 0.8 copy.38
  7.6 1.2 reduce-window.6
  8.7 0.2 slice_reduce_fusion
  9.3 1.9 convert_multiply_fusion.4
  11.2 0.2 fusion.18
  11.3 2.5 psum.14
  14.2 0.5 fusion.21
  14.7 3.1 %mul.214 = f32[256,2,1024]{2,1,0:T(2,128)} broadcast(bf16[256,1024]{1,0:T(8,128)(2,1)} %param.15), dimensions={0,2} | broadcast | bytes 2621440 | tf_op jit(solution)/shard_map/mul | solution.py:273
  17.8 3.7 %mul.215 = f32[512,1024]{1,0:T(8,128)} reshape(f32[256,2,1024]{2,1,0:T(2,128)} %mul.214) | data formatting | bytes 4194304 | tf_op jit(solution)/shard_map/mul | solution.py:273
  21.5 2.1 convolution_convert_fusion.refs_0_
  23.6 2.7 %fusion.9.refs_1_ = bf16[1024,1024]{1,0:T(8,128)(2,1)} fusion(f32[512,1024]{1,0:T(8,128)S(1)} %copy-done.13, f32[512]{0:T(512)S(1)} %mul.212, s32[512]{0:T(512)S(1)} %multiply_add_fusion), kind=kOutput, calls=%fused_computation.22 | convolution fusion | flops 1076363264 | bytes 4198400 | tf_op jit(solution)/shard_map/dot_general | solution.py:31
  26.4 1.0 fusion.42
  27.4 1.6 copy-done.2
  29.0 1.6 copy-done.3
  30.6 99.7 %dispatch.1 = (bf16[1024,2048]{1,0:T(8,128)(2,1)S(1)}, bf16[1024,2048]{1,0:T(8,128)(2,1)S(1)}, bf16[1024,512]{1,0:T(8,128)(2,1)S(1)}) custom-call(bf16[1024,1024]{1,0:T(8,128)(2,1)S(1)} %copy-done.2, bf16[1024,1024]{1,0:T(8,128)(2,1)S(1)} %copy-done.3, bf16[256,512]{1,0:T(8,128)(2,1)S(1)} %get-tuple-element.16.refs_2_), custom_call_target="tpu_custom_call" | custom-call | tf_op jit(solution)/shard_map/dispatch/pallas_call | solution.py:179
  130.3 2.3 fusion
  132.7 0.8 copy-done.12
  133.4 2.3 fusion.2
  135.8 3.0 %multiply_convert_fusion.1 = (bf16[1024,512]{1,0:T(8,128)(2,1)S(1)}, bf16[1024,512]{1,0:T(8,128)(2,1)S(1)}) fusion(f32[1024,512]{1,0:T(8,128)S(1)} %fusion, f32[1024,512]{1,0:T(8,128)S(1)} %fusion.2, bf16[1024,2048]{1,0:T(8,128)(2,1)S(1)} %get-tuple-element.11, bf16[1,512,2048]{2,1,0:T(8,128)(2,1)S(1)} %copy-done.28), kind=kOutput, calls=%fused_computation.13 | convolution fusion | flops 2154299392 | bytes 12582912 | tf_op jit(solution)/shard_map/dot_general | solution.py:41
  138.8 1.3 fusion.23
  140.1 1.3 add_convert_fusion.1
  141.4 0.2 collective-permute-start.1
  141.6 1.3 fusion.26
  142.9 1.3 add_convert_fusion.2
  144.2 4.4 %convolution_bitcast_fusion.1 = f32[1,2048,512]{2,1,0:T(8,128)} fusion(bf16[1024,2048]{1,0:T(8,128)(2,1)S(1)} %get-tuple-element.12, bf16[1024,512]{1,0:T(8,128)(2,1)S(1)} %get-tuple-element.18), kind=kOutput, calls=%fused_computation.4 | convolution fusion | flops 2147483648 | bytes 9437184 | tf_op jit(solution)/shard_map/dot_general | solution.py:35
  148.7 4.7 %convolution_bitcast_fusion = f32[1,512,2048]{2,1,0:T(8,128)} fusion(bf16[1024,2048]{1,0:T(8,128)(2,1)S(1)} %get-tuple-element.11, f32[1024,512]{1,0:T(8,128)S(1)} %fusion.2, f32[1024,512]{1,0:T(8,128)S(1)} %fusion), kind=kOutput, calls=%fused_computation.3 | convolution fusion | flops 2150629376 | bytes 12582912 | tf_op jit(solution)/shard_map/dot_general | solution.py:35
  153.4 1.0 add_convert_fusion.refs_0_
  154.4 42.4 %spread1.1 = bf16[1024,1024]{1,0:T(8,128)(2,1)S(1)} custom-call(bf16[1024,1024]{1,0:T(8,128)(2,1)S(1)} %add_convert_fusion.refs_0_), custom_call_target="tpu_custom_call" | custom-call | tf_op jit(solution)/shard_map/spread1/pallas_call | solution.py:235
  196.8 1.7 fusion.20
  198.5 14.2 %psum.15 = f32[256]{0:T(256)S(1)} all-reduce(f32[256]{0:T(256)S(1)} %get-tuple-element.27), channel_id=1, replica_groups=mesh['sp'=16,'tp'=2] {'tp'}, use_global_device_ids=true, to_apply=%region_7.8 | all-reduce | flops 256 | bytes 2048 | tf_op jit(solution)/shard_map/psum | solution.py:326
  212.7 1.8 fusion.17
  214.6 0.4 collective-permute-start.2
  215.0 6.6 %convolution_bitcast_fusion.2 = f32[1,2048,512]{2,1,0:T(8,128)} fusion(bf16[1024,2048]{1,0:T(8,128)(2,1)} %copy-done.4, bf16[1024,512]{1,0:T(8,128)(2,1)S(1)} %copy-done.9), kind=kOutput, calls=%fused_computation.5 | convolution fusion | flops 2147483648 | bytes 9437184 | tf_op jit(solution)/shard_map/dot_general | solution.py:35
  221.7 0.8 copy-done.16
  222.7 0.8 reshape.78
  223.5 0.4 copy.43
  223.9 0.2 copy.48
  224.1 14.2 %spread2.1 = bf16[1024,512]{1,0:T(8,128)(2,1)S(1)} custom-call(bf16[1024,512]{1,0:T(8,128)(2,1)S(1)} %bitcast.83), custom_call_target="tpu_custom_call" | custom-call | tf_op jit(solution)/shard_map/spread2/pallas_call | solution.py:235
  238.3 0.7 convolution_convert_fusion.1.refs_0_
  239.0 16.7 %spread3.1 = bf16[512,512]{1,0:T(8,128)(2,1)S(1)} custom-call(bf16[512,512]{1,0:T(8,128)(2,1)S(1)} %convolution_convert_fusion.1.refs_0_), custom_call_target="tpu_custom_call" | custom-call | tf_op jit(solution)/shard_map/spread3/pallas_call | solution.py:235
  255.8 1.4 multiply_convert_fusion.6
  257.2 1.4 collective-permute-start.3
  258.6 0.8 convert_reduce_fusion
  259.4 3.4 %collective-permute-done.3 = f32[2,512]{1,0:T(2,128)S(1)} collective-permute-done((f32[2,512]{1,0:T(2,128)S(1)}, f32[2,512]{1,0:T(2,128)S(1)}, u32[]{:S(2)}, u32[]{:S(2)}) %collective-permute-start.3) | collective-permute-done | bytes 4128 | tf_op jit(solution)/shard_map/ppermute | solution.py:17
  262.8 0.9 fusion.44
  263.8 0.8 fusion.43
  (78 shorter events, 1.4 us)
Async XLA Ops:
  0.6 129.7 %copy-start = (bf16[1,2048,512]{2,1,0:T(8,128)(2,1)S(1)}, bf16[1,2048,512]{2,1,0:T(8,128)(2,1)}, u32[]{:S(2)}) copy-start(bf16[1,2048,512]{2,1,0:T(8,128)(2,1)} %param.23) | copy-start | bytes 6291460
  0.6 13.3 %copy-start.25 = (s32[256,2]{0,1:T(2,128)S(1)}, s32[256,2]{0,1:T(2,128)}, u32[]{:S(2)}) copy-start(s32[256,2]{0,1:T(2,128)} %param.17) | copy-start | bytes 6148
  0.7 10.5 %copy-start.5 = (bf16[256,1024]{1,0:T(8,128)(2,1)S(1)}, bf16[256,1024]{1,0:T(8,128)(2,1)}, u32[]{:S(2)}) copy-start(bf16[256,1024]{1,0:T(8,128)(2,1)} %param.13) | copy-start | bytes 1572868
  0.7 13.2 %copy-start.27 = (f32[256,2]{0,1:T(2,128)S(1)}, f32[256,2]{0,1:T(2,128)}, u32[]{:S(2)}) copy-start(f32[256,2]{0,1:T(2,128)} %param.16) | copy-start | bytes 6148
  1.6 24.7 %collective-permute-start = (bf16[2,2,512]{2,1,0:T(2,128)(2,1)S(1)}, bf16[2,2,512]{2,1,0:T(2,128)(2,1)S(1)}, u32[]{:S(2)}, u32[]{:S(2)}) collective-permute-start(bf16[2,2,512]{2,1,0:T(2,128)(2,1)S(1)} %pad_maximum_fusion.3), channel_id=1, source_target_pairs={{0,2},{2,4},{4,6},{6,8},{8,10},{10,12},{12,14},{14,16},{16,18},{18... | collective-permute-start | bytes 12296 | tf_op jit(solution)/shard_map/ppermute | solution.py:17
  14.7 6.8 %copy-start.10 = (bf16[1024,256]{1,0:T(8,128)(2,1)}, bf16[1024,256]{1,0:T(8,128)(2,1)S(1)}, u32[]{:S(2)}) copy-start(bf16[1024,256]{1,0:T(8,128)(2,1)S(1)} %fusion.21) | copy-start | bytes 1572868
  17.8 3.7 %copy-start.24 = (f32[1024]{0:T(1024)S(1)}, f32[1024]{0:T(1024)}, u32[]{:S(2)}) copy-start(f32[1024]{0:T(1024)} %param.14) | copy-start | bytes 12292
  21.5 2.2 copy-start.13
  23.6 2.7 %copy-start.26 = (f32[3,512]{1,0:T(4,128)S(1)}, f32[3,512]{1,0:T(4,128)}, u32[]{:S(2)}) copy-start(f32[3,512]{1,0:T(4,128)} %param.21) | copy-start | bytes 18436
  23.6 2.7 %copy-start.15 = (f32[256,512]{1,0:T(8,128)S(1)}, f32[256,512]{1,0:T(8,128)}, u32[]{:S(2)}) copy-start(f32[256,512]{1,0:T(8,128)} %convert_multiply_fusion.4) | copy-start | bytes 1572868
  23.6 2.7 %copy-start.23 = (bf16[256,512]{1,0:T(8,128)(2,1)S(1)}, bf16[256,512]{1,0:T(8,128)(2,1)}, u32[]{:S(2)}) copy-start(bf16[256,512]{1,0:T(8,128)(2,1)} %param.19) | copy-start | bytes 786436
  27.4 1.6 copy-start.2
  29.0 1.6 copy-start.3
  130.3 13.9 %copy-start.4 = (bf16[1024,2048]{1,0:T(8,128)(2,1)}, bf16[1024,2048]{1,0:T(8,128)(2,1)S(1)}, u32[]{:S(2)}) copy-start(bf16[1024,2048]{1,0:T(8,128)(2,1)S(1)} %get-tuple-element.12) | copy-start | bytes 12582916
  130.3 3.1 %copy-start.12 = (bf16[1,2048,512]{2,1,0:T(8,128)(2,1)S(1)}, bf16[1,2048,512]{2,1,0:T(8,128)(2,1)}, u32[]{:S(2)}) copy-start(bf16[1,2048,512]{2,1,0:T(8,128)(2,1)} %param.24) | copy-start | bytes 6291460
  133.4 2.3 copy-start.28
  138.8 2.8 %copy-start.8 = (bf16[1024,512]{1,0:T(8,128)(2,1)}, bf16[1024,512]{1,0:T(8,128)(2,1)S(1)}, u32[]{:S(2)}) copy-start(bf16[1024,512]{1,0:T(8,128)(2,1)S(1)} %get-tuple-element.19) | copy-start | bytes 3145732
  141.4 11.9 %collective-permute-start.1 = (bf16[1024,1024]{1,0:T(8,128)(2,1)S(1)}, bf16[1024,1024]{1,0:T(8,128)(2,1)S(1)}, u32[]{:S(2)}, u32[]{:S(2)}) collective-permute-start(bf16[1024,1024]{1,0:T(8,128)(2,1)S(1)} %add_convert_fusion.1), channel_id=1, source_target_pairs={{0,1},{1,0},{2,3},{3,2},{4,5},{5,4},{6,7},{7,6},{8,9},{9,8},{10,11... | collective-permute-start | bytes 6291464 | tf_op jit(solution)/shard_map/ppermute | solution.py:320
  154.3 42.5 %copy-start.6 = (bf16[256,1024]{1,0:T(8,128)(2,1)S(1)}, bf16[256,1024]{1,0:T(8,128)(2,1)}, u32[]{:S(2)}) copy-start(bf16[256,1024]{1,0:T(8,128)(2,1)} %param.13) | copy-start | bytes 1572868
  154.3 42.5 %copy-start.11 = (bf16[1024,256]{1,0:T(8,128)(2,1)S(1)}, bf16[1024,256]{1,0:T(8,128)(2,1)}, u32[]{:S(2)}) copy-start(bf16[1024,256]{1,0:T(8,128)(2,1)} %copy-done.10) | copy-start | bytes 1572868
  196.8 15.9 %copy-start.7 = (bf16[256,1024]{1,0:T(8,128)(2,1)S(1)}, bf16[256,1024]{1,0:T(8,128)(2,1)}, u32[]{:S(2)}) copy-start(bf16[256,1024]{1,0:T(8,128)(2,1)} %param.13) | copy-start | bytes 1572868
  198.5 16.4 %copy-start.9 = (bf16[1024,512]{1,0:T(8,128)(2,1)S(1)}, bf16[1024,512]{1,0:T(8,128)(2,1)}, u32[]{:S(2)}) copy-start(bf16[1024,512]{1,0:T(8,128)(2,1)} %copy-done.8) | copy-start | bytes 3145732
  214.5 7.0 %copy-start.14 = (bf16[256,1024]{1,0:T(8,128)(2,1)}, bf16[256,1024]{1,0:T(8,128)(2,1)S(1)}, u32[]{:S(2)}) copy-start(bf16[256,1024]{1,0:T(8,128)(2,1)S(1)} %fusion.17) | copy-start | bytes 1572868
  214.6 7.0 %collective-permute-start.2 = (bf16[256,1024]{1,0:T(8,128)(2,1)S(1)}, bf16[256,1024]{1,0:T(8,128)(2,1)S(1)}, u32[]{:S(2)}, u32[]{:S(2)}) collective-permute-start(bf16[256,1024]{1,0:T(8,128)(2,1)S(1)} %fusion.17), channel_id=1, source_target_pairs={{0,1},{1,0},{2,3},{3,2},{4,5},{5,4},{6,7},{7,6},{8,9},{9,8},{10,11... | collective-permute-start | bytes 1572872 | tf_op jit(solution)/shard_map/ppermute | solution.py:332
  221.6 0.8 copy-start.16
  221.6 1.0 copy-start.18
  238.2 17.5 %copy-start.17 = (bf16[256,1024]{1,0:T(8,128)(2,1)S(1)}, bf16[256,1024]{1,0:T(8,128)(2,1)}, u32[]{:S(2)}) copy-start(bf16[256,1024]{1,0:T(8,128)(2,1)} %copy-done.16) | copy-start | bytes 1572868
  238.2 17.5 %copy-start.19 = (bf16[256,1024]{1,0:T(8,128)(2,1)S(1)}, bf16[256,1024]{1,0:T(8,128)(2,1)}, u32[]{:S(2)}) copy-start(bf16[256,1024]{1,0:T(8,128)(2,1)} %copy-done.18) | copy-start | bytes 1572868
  238.3 17.5 %copy-start.22 = (f32[256,512]{1,0:T(8,128)S(1)}, f32[256,512]{1,0:T(8,128)}, u32[]{:S(2)}) copy-start(f32[256,512]{1,0:T(8,128)} %get-tuple-element.17) | copy-start | bytes 1572868
  238.3 17.5 %copy-start.29 = (bf16[2048,512]{1,0:T(8,128)(2,1)S(1)}, bf16[2048,512]{1,0:T(8,128)(2,1)}, u32[]{:S(2)}) copy-start(bf16[2048,512]{1,0:T(8,128)(2,1)} %param.22) | copy-start | bytes 6291460
  255.8 7.1 %copy-start.20 = (bf16[256,512]{1,0:T(8,128)(2,1)S(1)}, bf16[256,512]{1,0:T(8,128)(2,1)}, u32[]{:S(2)}) copy-start(bf16[256,512]{1,0:T(8,128)(2,1)} %param.18) | copy-start | bytes 786436
  255.8 8.7 %copy-start.1 = (bf16[1,2048,512]{2,1,0:T(8,128)(2,1)S(1)}, bf16[1,2048,512]{2,1,0:T(8,128)(2,1)}, u32[]{:S(2)}) copy-start(bf16[1,2048,512]{2,1,0:T(8,128)(2,1)} %param.23) | copy-start | bytes 6291460
  257.2 6.5 %copy-start.21 = (bf16[256,512]{1,0:T(8,128)(2,1)S(1)}, bf16[256,512]{1,0:T(8,128)(2,1)}, u32[]{:S(2)}) copy-start(bf16[256,512]{1,0:T(8,128)(2,1)} %param.20) | copy-start | bytes 786436
  257.2 5.6 %collective-permute-start.3 = (f32[2,512]{1,0:T(2,128)S(1)}, f32[2,512]{1,0:T(2,128)S(1)}, u32[]{:S(2)}, u32[]{:S(2)}) collective-permute-start(f32[2,512]{1,0:T(2,128)S(1)} %slice.64), channel_id=1, source_target_pairs={{2,0},{4,2},{6,4},{8,6},{10,8},{12,10},{14,12},{16,14},{18,16},{20... | collective-permute-start | bytes 12296 | tf_op jit(solution)/shard_map/ppermute | solution.py:17
